TPU v7x, 1024 devices: a whole 4x8x16 slice. The times are simulated.
1024 devices in a mesh: rep: 16 (over z), fs: 8 (over y), tp: 8 (over x, core).
Axes of the slice: x: 4, y: 8, z: 16, core: 2. Of those that a mesh axis runs over, the one named last changes fastest.
Arguments:
- tokens: bfloat16 [6144, 2048], P('rep', ('fs', 'tp')), may hold values from -6 to 6
- cotangent: bfloat16 [6144, 2048], P('rep', ('fs', 'tp')), may hold values from -16 to 16
- gain: float32 [2048], replicated, may hold values from 0.1 to 1.9
- w_gate: bfloat16 [5376, 2048], P(('fs', 'tp')), may hold values from -0.125 to 0.125
- w_up: bfloat16 [5376, 2048], P(('fs', 'tp')), may hold values from -0.125 to 0.125
- w_down: bfloat16 [5376, 2048], P(('fs', 'tp')), may hold values from -0.078125 to 0.078125
Outputs:
- grad_input: bfloat16 [6144, 2048], P('rep', ('fs', 'tp'))
- grad_gain: float32 [2048], P(('fs', 'tp'))
- grad_gate: float32 [5376, 2048], P(('fs', 'tp'))
- grad_up: float32 [5376, 2048], P(('fs', 'tp'))
- grad_down: float32 [5376, 2048], P(('fs', 'tp'))
All inputs are finite; a program needn't handle non-finite values.
Results may differ from a plain program's by a relative error of at most 0.006.
Values may be sent and summed in bfloat16 or wider, within the bound.
No kernel may reach another device: no remote copies, remote signals or barrier semaphores. Data moves between devices by JAX's collectives and lax.ppermute only.
A program may use at most 64 MiB of HBM per device.

v0:
```python
import jax
import jax.numpy as jnp
from jax import lax
from jax.sharding import Mesh
from jax.sharding import PartitionSpec as P

FS_TP = ("fs", "tp_0", "tp_1")


EPS = 1e-06


def rows_first(arrays, axis, dims):
    turned = [jnp.moveaxis(a, dim, 0) for a, dim in zip(arrays, dims)]
    widths = [t[0].size for t in turned]
    both = jnp.concatenate([t.reshape(-1, w) for t, w in zip(turned, widths)], axis=1)
    whole = lax.all_gather(both, axis, axis=0, tiled=True)
    parts = jnp.split(whole, [sum(widths[:k]) for k in range(1, len(widths))], axis=1)
    return tuple(
        (
            jnp.moveaxis(b.reshape(-1, *t.shape[1:]), 0, dim)
            for b, t, dim in zip(parts, turned, dims)
        )
    )


def cut_along(x, dim, size):
    lengths = x.shape
    parts = x.reshape(*lengths[:dim], size, lengths[dim] // size, *lengths[dim + 1 :])
    return jnp.moveaxis(parts, dim, 0)


def sum_at_owner(x, axis, dim):
    size = lax.axis_size(axis)
    parts = lax.all_to_all(cut_along(x, dim, size), axis, 0, 0, tiled=True)
    return jnp.sum(parts, axis=0)


def over_axes(x, axes):
    for axis in axes:
        x = lax.psum(x, axis)
    return x


def right_product(left, weight):
    return lax.dot_general(
        left, weight, (((1,), (1,)), ((), ())), preferred_element_type=jnp.float32
    )


def left_product(left, right):
    return lax.dot_general(
        left, right, (((0,), (0,)), ((), ())), preferred_element_type=jnp.float32
    )


def local(tokens, cotangent, gain, w_gate, w_up, w_down):
    full_x, full_dy = rows_first((tokens, cotangent), FS_TP, (1, 1))
    xf = full_x.astype(jnp.float32)
    inv_rms = lax.rsqrt(jnp.mean(xf * xf, axis=1, keepdims=True) + EPS)
    unit = xf * inv_rms
    normed = (unit * gain).astype(jnp.bfloat16)
    gate = right_product(normed, w_gate)
    up = right_product(normed, w_up)
    sig = jax.nn.sigmoid(gate)
    active = gate * sig
    hidden = (active * up).astype(jnp.bfloat16)
    d_hidden = 0.5 * right_product(full_dy, w_down)
    d_gate = (d_hidden * up * sig * (1.0 + gate * (1.0 - sig))).astype(jnp.bfloat16)
    d_up = (d_hidden * active).astype(jnp.bfloat16)
    grad_down = 0.5 * left_product(hidden, full_dy)
    grad_gate = left_product(d_gate, normed)
    grad_up = left_product(d_up, normed)
    width = full_x.shape[1]
    partial_value = jnp.dot(d_gate, w_gate, preferred_element_type=jnp.float32) + jnp.dot(
        d_up, w_up, preferred_element_type=jnp.float32
    )
    summed = sum_at_owner(partial_value, FS_TP, 1)
    own_width = summed.shape[1]
    unit_own = tokens.astype(jnp.float32) * inv_rms
    gain_own = lax.dynamic_slice_in_dim(gain, lax.axis_index(FS_TP) * own_width, own_width, 0)
    d_unit = summed * gain_own
    row_mean = over_axes(jnp.sum(unit_own * d_unit, axis=1), FS_TP) / width
    gain_part = jnp.sum(unit_own * summed, axis=0)
    grad_gate, grad_up, grad_down, grad_gain = lax.psum(
        (grad_gate, grad_up, grad_down, gain_part), "rep"
    )
    grad_input = (
        cotangent.astype(jnp.float32) + inv_rms * (d_unit - unit_own * row_mean[:, None])
    ).astype(jnp.bfloat16)
    return (grad_input, grad_gain, grad_gate, grad_up, grad_down)


def solution(mesh):
    torus = Mesh(
        mesh.devices.reshape(mesh.shape["rep"], mesh.shape["fs"], 4, 2),
        ("rep", "fs", "tp_0", "tp_1"),
    )
    placed = (P("rep", FS_TP), P("rep", FS_TP), P(), P(FS_TP, None), P(FS_TP, None), P(FS_TP, None))
    return jax.shard_map(
        local,
        mesh=torus,
        in_specs=placed,
        out_specs=(P("rep", FS_TP), P(FS_TP), P(FS_TP, None), P(FS_TP, None), P(FS_TP, None)),
        check_vma=False,
    )
```

profile of v0, /device:TPU:6, one launch (start us, length us, event | category | flops | bytes accessed | tf_op | source)
XLA Modules:
  0.0 304.1 jit_solution(766373135430442699)
XLA Ops:
  7.2 0.0 copy-start
  7.2 0.0 copy-start.3
  7.2 0.0 all-gather.2.cloned.1.call-start
  7.2 1.5 pad_maximum_fusion
  8.7 0.0 all-gather.2.cloned.1.call-update
  8.7 105.0 %all-gather.2.cloned.1.call-done = bf16[2048,768]{1,0:T(8,128)(2,1)} async-done(((bf16[32,768]{1,0:T(8,128)(2,1)}), bf16[2048,768]{1,0:T(8,128)(2,1)}) %all-gather.2.cloned.1.call-update) | async-done | bytes 3145744 | tf_op jit(solution)/shard_map/all_gather | solution.py:17
  113.7 1.8 fusion
  115.5 0.0 copy-start.1
  115.5 0.0 copy-start.7
  115.6 2.0 fusion.2
  117.6 0.0 copy-done.3
  117.6 0.4 fusion.12
  118.0 0.0 copy-done
  118.0 0.4 fusion.13
  118.4 0.0 copy-done.1
  118.4 0.0 copy-done.7
  118.4 0.4 multiply_convert_fusion.1
  118.8 0.6 fusion.14
  119.4 2.3 convolution_add_fusion
  121.7 3.5 %copy.11 = f32[384,2048]{0,1:T(8,128)} copy(f32[384,2048]{1,0:T(8,128)} %convolution_add_fusion) | data formatting | bytes 6291456 | tf_op jit(solution)/shard_map/add | solution.py:75
  125.2 8.1 %all-to-all-start = ((f32[64,384,32]{1,2,0:T(8,128)}), f32[64,384,32]{1,2,0:T(8,128)}, u32[]{:S(2)}, u32[]{:S(2)}) async-start(f32[64,384,32]{1,2,0:T(8,128)} %bitcast.18), calls=%async_computation | async-start | bytes 6291456 | tf_op jit(solution)/shard_map/all_to_all | solution.py:35
  133.4 0.0 all-reduce.3.cloned.1.call-start
  133.4 0.0 copy-start.2
  133.4 1.6 fusion.15
  135.1 1.6 fusion.16
  136.7 0.0 copy-done.2
  136.7 1.6 convolution_multiply_fusion
  138.3 0.0 copy-start.5
  138.3 0.0 copy-start.6
  138.3 0.0 all-reduce.3.cloned.1.call-update
  138.3 0.8 dynamic_slice.3
  139.1 67.9 %all-to-all-done = f32[64,384,32]{1,2,0:T(8,128)} async-done(((f32[64,384,32]{1,2,0:T(8,128)}), f32[64,384,32]{1,2,0:T(8,128)}, u32[]{:S(2)}, u32[]{:S(2)}) %all-to-all-start) | async-done | bytes 3145760 | tf_op jit(solution)/shard_map/all_to_all | solution.py:35
  207.1 2.1 reduce_sum.37
  209.1 0.0 copy-done.5
  209.1 0.1 multiply_reduce_fusion
  209.3 32.9 %psum.52 = f32[32]{0:T(128)} all-reduce(f32[32]{0:T(128)S(1)} %get-tuple-element.5), channel_id=1, replica_groups=mesh['rep'=16,'fs'=8,'tp_0'=4,'tp_1'=2] {'rep'}, use_global_device_ids=true, to_apply=%region_7.0 | all-reduce | flops 32 | bytes 256 | tf_op jit(solution)/shard_map/psum | solution.py:85
  242.2 14.8 %psum.49 = f32[384]{0:T(512)S(1)} all-reduce(f32[384]{0:T(512)S(1)} %get-tuple-element.6), channel_id=1, replica_groups=mesh['rep'=16,'fs'=8,'tp_0'=4,'tp_1'=2] {'fs'}, use_global_device_ids=true, to_apply=%region_3.0 | all-reduce | flops 384 | bytes 3072 | tf_op jit(solution)/shard_map/psum | solution.py:41
  256.9 7.5 %psum.50 = f32[384]{0:T(512)S(1)} all-reduce(f32[384]{0:T(512)S(1)} %psum.49), channel_id=1, replica_groups=mesh['rep'=16,'fs'=8,'tp_0'=4,'tp_1'=2] {'tp_0'}, use_global_device_ids=true, to_apply=%region_4.0 | all-reduce | flops 384 | bytes 3072 | tf_op jit(solution)/shard_map/psum | solution.py:41
  264.4 2.4 psum.51
  266.9 0.0 copy-done.6
  266.9 0.7 add_convert_fusion
  267.5 24.7 %all-reduce.3.cloned.1.call-done = (f32[84,2048]{1,0:T(8,128)}, f32[84,2048]{1,0:T(8,128)}, f32[84,2048]{1,0:T(8,128)}) async-done(((f32[84,2048]{1,0:T(8,128)}, f32[84,2048]{1,0:T(8,128)}, f32[84,2048]{1,0:T(8,128)}), (f32[84,2048]{1,0:T(8,128)}, f32[84,2048]{1,0:T(8,128)}, f32[84,2048]{1,0:T(8,128)})) %all-reduce.3.cloned.1.call-update) | async-done | bytes 2064400 | tf_op jit(solution)/shard_map/psum | solution.py:85
  292.2 0.0 copy-start.4
  292.2 2.1 copy.15
  294.3 2.0 copy.16
  296.4 0.0 copy-done.4
  296.4 0.9 copy.17
  (2 shorter events, 0.0 us)
Async XLA Ops:
  7.2 110.8 %copy-start = (bf16[84,2048]{1,0:T(8,128)(2,1)S(1)}, bf16[84,2048]{1,0:T(8,128)(2,1)}, u32[]{:S(2)}) copy-start(bf16[84,2048]{1,0:T(8,128)(2,1)} %param.9) | copy-start | bytes 1032196
  7.2 110.4 %copy-start.3 = (bf16[84,2048]{1,0:T(8,128)(2,1)S(1)}, bf16[84,2048]{1,0:T(8,128)(2,1)}, u32[]{:S(2)}) copy-start(bf16[84,2048]{1,0:T(8,128)(2,1)} %param.10) | copy-start | bytes 1032196
  7.2 106.5 %all-gather.2.cloned.1.call-start = ((), (), s32[]{:S(2)}) async-start(), calls=%async_computation.1 | async-start | bytes 3194880 | tf_op jit(solution)/shard_map/all_gather | solution.py:17
  115.5 2.8 copy-start.1
  115.5 2.8 copy-start.7
  125.2 81.8 %all-to-all-start = ((f32[64,384,32]{1,2,0:T(8,128)}), f32[64,384,32]{1,2,0:T(8,128)}, u32[]{:S(2)}, u32[]{:S(2)}) async-start(f32[64,384,32]{1,2,0:T(8,128)} %bitcast.18), calls=%async_computation | async-start | bytes 6291456 | tf_op jit(solution)/shard_map/all_to_all | solution.py:35
  133.4 158.8 %all-reduce.3.cloned.1.call-start = ((), (), s32[]{:S(2)}) async-start(), calls=%async_computation.2 | async-start | bytes 4325376 | tf_op jit(solution)/shard_map/psum | solution.py:85
  133.4 3.3 %copy-start.2 = (bf16[2048,768]{1,0:T(8,128)(2,1)S(1)}, bf16[2048,768]{1,0:T(8,128)(2,1)}, u32[]{:S(2)}) copy-start(bf16[2048,768]{1,0:T(8,128)(2,1)} %all-gather.2.cloned.1.call-done) | copy-start | bytes 9437188
  138.3 70.8 %copy-start.5 = (bf16[384,32]{0,1:T(8,128)(2,1)S(1)}, bf16[384,32]{0,1:T(8,128)(2,1)}, u32[]{:S(2)}) copy-start(bf16[384,32]{0,1:T(8,128)(2,1)} %param.6) | copy-start | bytes 73732
  138.3 128.5 %copy-start.6 = (bf16[384,32]{0,1:T(8,128)(2,1)S(1)}, bf16[384,32]{0,1:T(8,128)(2,1)}, u32[]{:S(2)}) copy-start(bf16[384,32]{0,1:T(8,128)(2,1)} %param.7) | copy-start | bytes 73732
  292.2 4.1 %copy-start.4 = (f32[84,2048]{1,0:T(8,128)S(1)}, f32[84,2048]{1,0:T(8,128)}, u32[]{:S(2)}) copy-start(f32[84,2048]{1,0:T(8,128)} %get-tuple-element.16) | copy-start | bytes 2064388
Sparse Core Ops, SparseCore 0:
  13.1 100.5 all-gather.1
  138.5 153.7 all-reduce.2
where the time goes:
time: 305 us; the launch traced here: 304 us
  waiting for transfers between devices  198 us (65%)
  blocking collectives  57.6 us (19%)
  between operations  14.2 us (5%)
  local copies, waits for them, and re-layouts  9.32 us (3%)
  matrix products  8.93 us (3%)
  starting transfers between devices  8.22 us (3%)
  other arithmetic  8.17 us (3%)
    all_gather x1, waiting for transfers between devices, rows_first(): whole = lax.all_gather(both, axis, axis=0, tiled=True)  105 us
    all_to_all x1, waiting for transfers between devices, sum_at_owner(): parts = lax.all_to_all(cut_along(x, dim, size), axis, 0, 0, tiled=True)  67.9 us
    psum x1, blocking collectives, local(): lax.psum((grad_gate, grad_up, grad_down, gain_part), 'rep')  32.9 us
    psum x1, waiting for transfers between devices, local(): lax.psum((grad_gate, grad_up, grad_down, gain_part), 'rep')  24.7 us
    psum x3, blocking collectives, over_axes(): x = lax.psum(x, axis)  24.7 us
    all_to_all x1, starting transfers between devices, sum_at_owner(): parts = lax.all_to_all(cut_along(x, dim, size), axis, 0, 0, tiled=True)  8.15 us
  transfers between devices with their start and end apart: 3, of which 3 were waited for; matrix products, arithmetic and copies ran while one was open for 3% of the time, Pallas kernels for 0%

commit v1 on v0

v1 whole, which is shorter than its diff:
```python
import functools

import jax
import jax.numpy as jnp
from jax import lax
from jax.experimental import pallas as pl
from jax.experimental.pallas import tpu as pltpu
from jax.sharding import Mesh
from jax.sharding import PartitionSpec as P


FS_TP = ("fs", "tp_0", "tp_1")
EPS = 1e-06
BF = jnp.bfloat16
F32 = jnp.float32
LANES = 128
VMEM = pl.BlockSpec(memory_space=pltpu.VMEM)
ANY = pl.BlockSpec(memory_space=pl.ANY)


def sigmoid(v):
    return jax.nn.sigmoid(v)


def gain_columns(gain_ref, out_ref):
    for q in range(gain_ref.shape[0]):
        row = jnp.broadcast_to(gain_ref[q : q + 1, :], (LANES, LANES))
        out_ref[q * LANES : (q + 1) * LANES, :] = row.T


def main_kernel(
    sizes,
    own_ref,
    other_ref,
    gate_w_ref,
    up_w_ref,
    down_w_ref,
    gain_ref,
    part_ref,
    inv_ref,
    *rest,
):
    n_fs, n_x, n_core, tokens, hidden, padded, width, block = sizes
    n_pieces = 3 * (width // LANES)
    pieces = rest[:n_pieces]
    normed_s, cot_s, pair_s, down_s, delta_s, hidden_s, gain_s = rest[n_pieces:]
    core = lax.axis_index("tp_1")

    low = padded - 16
    pair_s[low:padded, :] = jnp.zeros((16, width), BF)
    pair_s[padded + low : 2 * padded, :] = jnp.zeros((16, width), BF)
    down_s[low:padded, :] = jnp.zeros((16, width), BF)
    pair_s[0:hidden, :] = gate_w_ref[...]
    pair_s[padded : padded + hidden, :] = up_w_ref[...]
    down_s[0:hidden, :] = down_w_ref[...]
    gain_columns(gain_ref, gain_s)

    def square_sum(s, acc):
        for ref in (own_ref, other_ref):
            v = ref[s, :, 0:tokens].astype(F32)
            v = v * v
            for k in range(block // 8):
                acc = acc + v[8 * k : 8 * k + 8, :]
        return acc

    total = lax.fori_loop(0, n_fs * n_x, square_sum, jnp.zeros((8, tokens), F32))
    mean = jnp.sum(total, axis=0, keepdims=True) / width
    inv = lax.rsqrt(mean + EPS)
    inv_ref[...] = jnp.broadcast_to(inv, (8, tokens))

    def normalise(s, carry):
        x = s // n_fs
        y = s % n_fs
        for ref, which in ((own_ref, core), (other_ref, 1 - core)):
            at = pl.multiple_of(((y * n_x + x) * n_core + which) * block, block)
            v = ref[s, :, 0:tokens].astype(F32) * inv
            g = gain_s[pl.ds(at, block), :]
            v = v * jnp.concatenate([g] * (tokens // LANES), axis=1)
            normed_s[pl.ds(at, block), :] = v.astype(BF)
            cot_s[pl.ds(at, block), :] = ref[s, :, tokens : 2 * tokens]
        return carry

    lax.fori_loop(0, n_fs * n_x, normalise, 0)

    both = jnp.dot(pair_s[...], normed_s[...], preferred_element_type=F32)
    d_hidden = 0.5 * jnp.dot(down_s[...], cot_s[...], preferred_element_type=F32)
    gate = both[0:padded, :]
    up = both[padded : 2 * padded, :]
    sig = sigmoid(gate)
    active = gate * sig
    hidden_s[...] = (active * up).astype(BF)
    d_gate = (d_hidden * up * sig * (1.0 + gate * (1.0 - sig))).astype(BF)
    d_up = (d_hidden * active).astype(BF)
    delta_s[0:padded, :] = d_gate
    delta_s[padded : 2 * padded, :] = d_up
    row = jnp.sum(d_gate.astype(F32) * gate + d_up.astype(F32) * up, axis=0, keepdims=True)
    high = row.astype(BF)
    rest_of = (row - high.astype(F32)).astype(BF)
    tail = jnp.concatenate(
        [high, rest_of, jnp.zeros((part_ref.shape[1] - block - 2, tokens), BF)], axis=0
    )
    for d in range(part_ref.shape[0]):
        part_ref[d, block:, :] = tail

    step = 256
    for b in range(width // step):
        cols = slice(b * step, (b + 1) * step)
        value = lax.dot_general(
            pair_s[:, cols], delta_s[...], (((0,), (0,)), ((), ())), preferred_element_type=F32
        ).astype(BF)
        for k in range(step // block):
            part_ref[b * (step // block) + k, 0:block, :] = value[k * block : (k + 1) * block, :]
    for b in range(width // step):
        rows = slice(b * step, (b + 1) * step)
        two = lax.dot_general(
            delta_s[...], normed_s[rows, :], (((1,), (1,)), ((), ())), preferred_element_type=F32
        )
        one = 0.5 * lax.dot_general(
            hidden_s[...], cot_s[rows, :], (((1,), (1,)), ((), ())), preferred_element_type=F32
        )
        for k in range(step // LANES):
            at = b * (step // LANES) + k
            lanes = slice(k * LANES, (k + 1) * LANES)
            pieces[at][...] = two[0:hidden, lanes]
            pieces[width // LANES + at][...] = two[padded : padded + hidden, lanes]
            pieces[2 * (width // LANES) + at][...] = one[0:hidden, lanes]


def weight_kernel(n_blocks, gate_w_ref, up_w_ref, gain_ref, one_ref, after_ref, *rest):
    pieces = rest[: 3 * n_blocks]
    gate_ref, up_ref, down_ref, slab_ref = rest[3 * n_blocks :]
    per = slab_ref.shape[0] // n_blocks
    for b in range(n_blocks):
        lanes = slice(b * LANES, (b + 1) * LANES)
        g, u = pieces[b][...], pieces[n_blocks + b][...]
        gate_ref[:, lanes] = g
        up_ref[:, lanes] = u
        down_ref[:, lanes] = pieces[2 * n_blocks + b][...]
        v = g * gate_w_ref[:, lanes].astype(F32) + u * up_w_ref[:, lanes].astype(F32)
        v = jnp.sum(v, axis=0, keepdims=True) / gain_ref[b : b + 1, :]
        v = jnp.broadcast_to(v, (8, LANES))
        for k in range(per):
            slab_ref[b * per + k] = v


def input_kernel(block, n_x, n_core, width, part_ref, tok_ref, cot_ref, inv_ref, gain_ref, out_ref, gain_s):
    sources, rows, tokens = part_ref.shape
    me = (lax.axis_index("fs") * n_x + lax.axis_index("tp_0")) * n_core + lax.axis_index("tp_1")
    gain_columns(gain_ref, gain_s)

    def add(s, acc):
        return acc + part_ref[s].astype(F32)

    total = lax.fori_loop(0, sources, add, jnp.zeros((rows, tokens), F32))
    summed = total[0:block, :]
    row = (total[block : block + 1, :] + total[block + 1 : block + 2, :]) / width
    inv = inv_ref[0:1, :]
    g = gain_s[pl.ds(pl.multiple_of(me * block, block), block), :]
    d_unit = summed * jnp.concatenate([g] * (tokens // LANES), axis=1)
    unit = tok_ref[...].astype(F32) * inv
    out_ref[...] = (cot_ref[...].astype(F32) + inv * (d_unit - unit * row)).astype(BF)


def spread(block, axis):
    n = lax.axis_size(axis)
    copies = jnp.broadcast_to(block[None], (n,) + block.shape)
    return lax.all_to_all(copies, axis, 0, 0, tiled=True)


def body(tokens, cotangent, gain, w_gate, w_up, w_down):
    n_fs, n_x, n_core = (lax.axis_size(a) for a in FS_TP)
    members = n_fs * n_x * n_core
    rows, block = tokens.shape
    width = gain.shape[0]
    hidden = w_gate.shape[0]
    padded = -(-hidden // 32) * 32
    n_blocks = width // LANES
    tok_t, cot_t = tokens.T, cotangent.T
    both = jnp.concatenate([tok_t, cot_t], axis=1)
    column = spread(both, "fs")
    plane = spread(column.reshape(n_fs * block, 2 * rows), "tp_0")
    plane = plane.reshape(n_fs * n_x, block, 2 * rows)
    other = lax.ppermute(plane, "tp_1", [(0, 1), (1, 0)])
    gain_rows = gain.reshape(n_blocks, LANES)

    sizes = (n_fs, n_x, n_core, rows, hidden, padded, width, block)
    outs = pl.pallas_call(
        functools.partial(main_kernel, sizes),
        out_shape=[
            jax.ShapeDtypeStruct((members, block + 8, rows), BF),
            jax.ShapeDtypeStruct((8, rows), F32),
        ]
        + [jax.ShapeDtypeStruct((hidden, LANES), F32)] * (3 * n_blocks),
        in_specs=[VMEM] * 6,
        out_specs=[VMEM] * (2 + 3 * n_blocks),
        scratch_shapes=[
            pltpu.VMEM((width, rows), BF),
            pltpu.VMEM((width, rows), BF),
            pltpu.VMEM((2 * padded, width), BF),
            pltpu.VMEM((padded, width), BF),
            pltpu.VMEM((2 * padded, rows), BF),
            pltpu.VMEM((padded, rows), BF),
            pltpu.VMEM((width, LANES), F32),
        ],
        compiler_params=pltpu.CompilerParams(vmem_limit_bytes=30 * 2**20),
        cost_estimate=pl.CostEstimate(flops=11 * 10**8, bytes_accessed=10**7, transcendentals=0),
        name="main",
    )(plane, other, w_gate, w_up, w_down, gain_rows)
    part, inv, pieces = outs[0], outs[1], outs[2:]

    parts = lax.all_to_all(part, FS_TP, 0, 0, tiled=True)
    one = inv[0:1, 0:1]
    *pieces, one = lax.psum((*pieces, one), "rep")

    grad_gate, grad_up, grad_down, slabs = pl.pallas_call(
        functools.partial(weight_kernel, n_blocks),
        out_shape=[jax.ShapeDtypeStruct((hidden, width), F32)] * 3
        + [jax.ShapeDtypeStruct((members, 8, LANES), F32)],
        in_specs=[VMEM] * 4 + [ANY] + [VMEM] * (3 * n_blocks),
        out_specs=[VMEM] * 4,
        compiler_params=pltpu.CompilerParams(vmem_limit_bytes=20 * 2**20),
        name="weights",
    )(w_gate, w_up, gain_rows, one, parts, *pieces)

    slabs = lax.all_to_all(slabs, FS_TP, 0, 0, tiled=True)
    grad_input = pl.pallas_call(
        functools.partial(input_kernel, block, n_x, n_core, width),
        out_shape=jax.ShapeDtypeStruct((block, rows), BF),
        in_specs=[VMEM] * 5,
        out_specs=VMEM,
        scratch_shapes=[pltpu.VMEM((width, LANES), F32)],
        compiler_params=pltpu.CompilerParams(vmem_limit_bytes=20 * 2**20),
        cost_estimate=pl.CostEstimate(flops=10**8, bytes_accessed=2 * 10**6, transcendentals=0),
        name="input",
    )(parts, tok_t, cot_t, inv, gain_rows)
    me = lax.axis_index(FS_TP) % (LANES // block)
    grad_gain = lax.dynamic_slice_in_dim(jnp.sum(slabs[:, 0, :], axis=0), me * block, block, 0)
    return (grad_input.T, grad_gain, grad_gate, grad_up, grad_down)


def solution(mesh):
    torus = Mesh(
        mesh.devices.reshape(mesh.shape["rep"], mesh.shape["fs"], 4, 2),
        ("rep", "fs", "tp_0", "tp_1"),
    )
    placed = (P("rep", FS_TP), P("rep", FS_TP), P(), P(FS_TP, None), P(FS_TP, None), P(FS_TP, None))
    return jax.shard_map(
        body,
        mesh=torus,
        in_specs=placed,
        out_specs=(P("rep", FS_TP), P(FS_TP), P(FS_TP, None), P(FS_TP, None), P(FS_TP, None)),
        check_vma=False,
    )
```

time: 305 us -> 235 us (0.77); the launches traced: 304 us -> 230 us
  waiting for transfers between devices: 198 us -> 13 us
  blocking collectives: 57.6 us -> 132 us
  local copies, waits for them, and re-layouts: 9.32 us -> 56.3 us
  between operations: 14.2 us -> 0.86 us
  starting transfers between devices: 8.22 us -> 18.9 us
  matrix products: 8.93 us -> 0 us
  Pallas kernels: 0 us -> 7.98 us
  other arithmetic: 8.17 us -> 0.85 us
    all_gather x1 -> x0, waiting for transfers between devices: 105 us -> none  [rows_first(): whole = lax.all_gather(both, axis, axis=0, tiled=True)]
    all_to_all x1 -> x2, waiting for transfers between devices: 67.9 us -> 9.58 us  [the longest x1 9.58 us: body(): slabs = lax.all_to_all(slabs, FS_TP, 0, 0, tiled=True)]
    unnamed x19 -> x172, local copies, waits for them, and re-layouts: 5.01 us -> 55.1 us
    all_to_all x0 -> x2, blocking collectives: none -> 43.5 us  [spread(): return lax.all_to_all(copies, axis, 0, 0, tiled=True)]
    psum x4 -> x1, blocking collectives: 57.6 us -> 88.7 us  [body(): *pieces, one = lax.psum((*pieces, one), 'rep')]
    psum x1 -> x0, waiting for transfers between devices: 24.7 us -> none  [local(): lax.psum((grad_gate, grad_up, grad_down, gain_part), 'rep')]
    dot_general x8 -> x0, matrix products: 8.93 us -> none  [the longest x3 4.86 us: left_product(): lax.dot_general(left, right, (((0,), (0,)), ((), ())), preferred_element_...]
    all_to_all x1 -> x2, starting transfers between devices: 8.15 us -> 17 us  [the longest x1 10.8 us: body(): slabs = lax.all_to_all(slabs, FS_TP, 0, 0, tiled=True)]
  transfers between devices with their start and end apart: 3 -> 3, of which waited for: 3 -> 2; matrix products, arithmetic and copies ran while one was open for 3% -> 0% of each run, Pallas kernels for 0% -> 1%
where the time goes in v1:
time: 235 us; the launch traced here: 230 us
  blocking collectives  132 us (56%)
  local copies, waits for them, and re-layouts  56.3 us (24%)
  starting transfers between devices  18.9 us (8%)
  waiting for transfers between devices  13 us (6%)
  Pallas kernels  7.98 us (3%)
    psum x1, blocking collectives, body(): *pieces, one = lax.psum((*pieces, one), 'rep')  88.7 us
    unnamed x172, local copies, waits for them, and re-layouts  55.1 us
    all_to_all x2, blocking collectives, spread(): return lax.all_to_all(copies, axis, 0, 0, tiled=True)  43.5 us
    all_to_all x1, starting transfers between devices, body(): slabs = lax.all_to_all(slabs, FS_TP, 0, 0, tiled=True)  10.8 us
    all_to_all x1, waiting for transfers between devices, body(): slabs = lax.all_to_all(slabs, FS_TP, 0, 0, tiled=True)  9.58 us
    all_to_all x1, starting transfers between devices, body(): parts = lax.all_to_all(part, FS_TP, 0, 0, tiled=True)  6.22 us
  transfers between devices with their start and end apart: 3, of which 2 were waited for; matrix products, arithmetic and copies ran while one was open for 0% of the time, Pallas kernels for 1%

profile of v1, /device:TPU:6, one launch (start us, length us, event | category | flops | bytes accessed | tf_op | source)
XLA Modules:
  0.0 230.1 jit_solution(5270516020176401237)
XLA Ops:
  0.6 0.8 pad_maximum_fusion
  1.4 21.6 %all_to_all.20 = bf16[8,32,768]{2,1,0:T(8,128)(2,1)S(1)} all-to-all(bf16[8,32,768]{2,1,0:T(8,128)(2,1)S(1)} %broadcast_in_dim.6), channel_id=1, replica_groups=mesh['rep'=16,'fs'=8,'tp_0'=4,'tp_1'=2] {'fs'}, dimensions={0} | all-to-all | bytes 786432 | tf_op jit(solution)/shard_map/all_to_all | solution.py:167
  23.2 22.0 %all_to_all.21 = bf16[4,256,768]{2,1,0:T(8,128)(2,1)S(1)} all-to-all(bf16[4,256,768]{2,1,0:T(8,128)(2,1)S(1)} %broadcast_in_dim.15), channel_id=1, replica_groups=mesh['rep'=16,'fs'=8,'tp_0'=4,'tp_1'=2] {'tp_0'}, dimensions={0} | all-to-all | bytes 3145728 | tf_op jit(solution)/shard_map/all_to_all | solution.py:167
  45.1 1.9 collective-permute-start
  47.0 3.4 %collective-permute-done.other_ref = bf16[32,32,768]{2,1,0:T(8,128)(2,1)S(1)} collective-permute-done((bf16[32,32,768]{2,1,0:T(8,128)(2,1)S(1)}, bf16[32,32,768]{2,1,0:T(8,128)(2,1)S(1)}, u32[]{:S(2)}, u32[]{:S(2)}) %collective-permute-start) | collective-permute-done | bytes 1572896 | tf_op jit(solution)/shard_map/ppermute | solution.py:183
  50.4 4.0 %main.1 = (bf16[64,40,384]{2,1,0:T(8,128)(2,1)S(1)}, f32[8,384]{1,0:T(8,128)S(1)}, f32[84,128]{1,0:T(8,128)S(1)}, f32[84,128]{1,0:T(8,128)S(1)}, f32[84,128]{1,0...) custom-call(bf16[32,32,768]{2,1,0:T(8,128)(2,1)S(1)} %bitcast.7, ...), custom_call_target="tpu_custom_call" | custom-call | flops 1100000000 | bytes 10000000 | tf_op jit(solution)/shard_map/main/pallas_call | solution.py:187
  54.5 1.3 copy-done
  62.5 0.6 copy-done.48
  70.5 0.6 copy-done.61
  72.4 0.6 copy-done.64
  82.8 0.6 copy-done.81
  84.6 6.2 %all-to-all-start.2 = ((bf16[64,40,384]{2,1,0:T(8,128)(2,1)}), bf16[64,40,384]{2,1,0:T(8,128)(2,1)S(1)}, u32[]{:S(2)}, u32[]{:S(2)}) async-start(bf16[64,40,384]{2,1,0:T(8,128)(2,1)} %copy-done), calls=%async_computation.2 | async-start | bytes 3932160 | tf_op jit(solution)/shard_map/all_to_all | solution.py:211
  92.0 88.7 %all-reduce.2 = (f32[1,1]{1,0:T(1,128)}, f32[84,128]{1,0:T(8,128)S(1)}, f32[84,128]{1,0:T(8,128)S(1)}, f32[84,128]{1,0:T(8,128)S(1)}, f32[84,128]{1,0:T(8,128)S(...) all-reduce(f32[1,1]{1,0:T(1,128)} %slice.6, ...), channel_id=1, replica_groups=mesh['rep'=16,'fs'=8,'tp_0'=4,'tp_1'=2] {'rep'}, use_global_device_ids=true, to_apply=%region_0.0 | all-reduce | flops 516097 | bytes 4128776 | tf_op jit(solution)/shard_map/psum | solution.py:213
  180.7 0.8 copy-done.7
  181.5 0.8 copy-done.8
  182.3 0.8 copy-done.9
  183.1 0.8 copy-done.10
  183.9 0.8 copy-done.11
  184.7 0.8 copy-done.12
  185.4 0.8 copy-done.13
  186.2 0.8 copy-done.14
  187.0 0.8 copy-done.15
  187.8 0.8 copy-done.16
  188.6 0.8 copy-done.17
  189.4 0.8 copy-done.18
  190.2 0.8 copy-done.19
  191.0 0.8 copy-done.20
  191.8 0.8 copy-done.21
  192.5 0.8 copy-done.22
  193.3 0.8 copy-done.23
  194.1 0.8 copy-done.24
  194.9 0.8 copy-done.25
  195.7 0.8 copy-done.26
  196.5 0.8 copy-done.27
  197.3 0.8 copy-done.28
  198.1 0.8 copy-done.29
  198.9 0.8 copy-done.30
  199.6 0.8 copy-done.31
  200.4 0.8 copy-done.32
  201.2 0.8 copy-done.33
  202.0 0.8 copy-done.34
  202.8 0.8 copy-done.35
  203.6 0.8 copy-done.36
  204.4 2.4 %weights.1 = (f32[84,2048]{1,0:T(8,128)}, f32[84,2048]{1,0:T(8,128)}, f32[84,2048]{1,0:T(8,128)}, f32[64,8,128]{2,1,0:T(8,128)}) custom-call(bf16[84,2048]{1,0:T(8,128)(2,1)S(1)} %copy-done.1, bf16[84,2048]{1,0:T(8,128)(2,1)S(1)} %copy-done.2, f32[16,128]{1,0:T(8,128)S(1)} %bitcast.13, f32[1,1]{1,0:T(1,128)} %get-tuple-element.113.one_ref, ...), custom_call_target="tpu_custom_call" | custom-call | tf_op jit(solution)/shard_map/weights/pallas_call | solution.py:215
  206.7 10.8 %all-to-all-start.3 = ((f32[64,8,128]{2,1,0:T(8,128)}), f32[64,8,128]{2,1,0:T(8,128)S(1)}, u32[]{:S(2)}, u32[]{:S(2)}) async-start(f32[64,8,128]{2,1,0:T(8,128)} %get-tuple-element.109), calls=%async_computation.3 | async-start | bytes 524288 | tf_op jit(solution)/shard_map/all_to_all | solution.py:225
  217.6 0.7 copy-done.85
  218.3 1.6 input.1
  219.9 9.6 %all-to-all-done.3 = f32[64,8,128]{2,1,0:T(8,128)S(1)} async-done(((f32[64,8,128]{2,1,0:T(8,128)}), f32[64,8,128]{2,1,0:T(8,128)S(1)}, u32[]{:S(2)}, u32[]{:S(2)}) %all-to-all-start.3) | async-done | bytes 262176 | tf_op jit(solution)/shard_map/all_to_all | solution.py:225
  (142 shorter events, 28.4 us)
Async XLA Ops:
  23.1 27.3 %copy-start.1 = (bf16[84,2048]{1,0:T(8,128)(2,1)S(1)}, bf16[84,2048]{1,0:T(8,128)(2,1)}, u32[]{:S(2)}) copy-start(bf16[84,2048]{1,0:T(8,128)(2,1)} %gate_w_ref.3) | copy-start | bytes 1032196
  23.1 27.3 %copy-start.2 = (bf16[84,2048]{1,0:T(8,128)(2,1)S(1)}, bf16[84,2048]{1,0:T(8,128)(2,1)}, u32[]{:S(2)}) copy-start(bf16[84,2048]{1,0:T(8,128)(2,1)} %up_w_ref.3) | copy-start | bytes 1032196
  23.1 27.3 %copy-start.3 = (bf16[84,2048]{1,0:T(8,128)(2,1)S(1)}, bf16[84,2048]{1,0:T(8,128)(2,1)}, u32[]{:S(2)}) copy-start(bf16[84,2048]{1,0:T(8,128)(2,1)} %down_w_ref.1) | copy-start | bytes 1032196
  23.2 27.3 %copy-start.6 = (f32[2048]{0:T(1024)S(1)}, f32[2048]{0:T(1024)}, u32[]{:S(2)}) copy-start(f32[2048]{0:T(1024)} %param.8) | copy-start | bytes 24580
  45.1 5.3 %collective-permute-start = (bf16[32,32,768]{2,1,0:T(8,128)(2,1)S(1)}, bf16[32,32,768]{2,1,0:T(8,128)(2,1)S(1)}, u32[]{:S(2)}, u32[]{:S(2)}) collective-permute-start(bf16[32,32,768]{2,1,0:T(8,128)(2,1)S(1)} %bitcast.6), channel_id=1, source_target_pairs={{0,1},{1,0},{2,3},{3,2},{4,5},{5,4},{6,7},{7,6},{8,9},{9,8},{10,11... | collective-permute-start | bytes 4718600 | tf_op jit(solution)/shard_map/ppermute | solution.py:183
  54.5 1.3 copy-start
  55.7 0.6 copy-start.37
  56.4 0.6 copy-start.38
  58.2 0.6 copy-start.41
  62.5 0.6 copy-start.48
  70.5 0.6 copy-start.61
  72.4 0.6 copy-start.64
  82.8 0.6 copy-start.81
  84.6 96.1 %all-to-all-start.2 = ((bf16[64,40,384]{2,1,0:T(8,128)(2,1)}), bf16[64,40,384]{2,1,0:T(8,128)(2,1)S(1)}, u32[]{:S(2)}, u32[]{:S(2)}) async-start(bf16[64,40,384]{2,1,0:T(8,128)(2,1)} %copy-done), calls=%async_computation.2 | async-start | bytes 3932160 | tf_op jit(solution)/shard_map/all_to_all | solution.py:211
  180.7 0.8 copy-start.7
  181.5 0.8 copy-start.8
  182.3 0.8 copy-start.9
  183.1 0.8 copy-start.10
  183.9 0.8 copy-start.11
  184.7 0.8 copy-start.12
  185.4 0.8 copy-start.13
  186.2 0.8 copy-start.14
  187.0 0.8 copy-start.15
  187.8 0.8 copy-start.16
  188.6 0.8 copy-start.17
  189.4 0.8 copy-start.18
  190.2 0.8 copy-start.19
  191.0 0.8 copy-start.20
  191.8 0.8 copy-start.21
  192.5 0.8 copy-start.22
  193.3 0.8 copy-start.23
  194.1 0.8 copy-start.24
  194.9 0.8 copy-start.25
  195.7 0.8 copy-start.26
  196.5 0.8 copy-start.27
  197.3 0.8 copy-start.28
  198.1 0.8 copy-start.29
  198.9 0.8 copy-start.30
  199.6 0.8 copy-start.31
  200.4 0.8 copy-start.32
  201.2 0.8 copy-start.33
  202.0 0.8 copy-start.34
  202.8 0.8 copy-start.35
  203.6 0.8 copy-start.36
  204.4 13.2 %copy-start.4 = (bf16[384,32]{0,1:T(8,128)(2,1)S(1)}, bf16[384,32]{0,1:T(8,128)(2,1)}, u32[]{:S(2)}) copy-start(bf16[384,32]{0,1:T(8,128)(2,1)} %param.7) | copy-start | bytes 73732
  204.4 13.2 %copy-start.5 = (bf16[384,32]{0,1:T(8,128)(2,1)S(1)}, bf16[384,32]{0,1:T(8,128)(2,1)}, u32[]{:S(2)}) copy-start(bf16[384,32]{0,1:T(8,128)(2,1)} %param.6) | copy-start | bytes 73732
  206.7 22.7 %all-to-all-start.3 = ((f32[64,8,128]{2,1,0:T(8,128)}), f32[64,8,128]{2,1,0:T(8,128)S(1)}, u32[]{:S(2)}, u32[]{:S(2)}) async-start(f32[64,8,128]{2,1,0:T(8,128)} %get-tuple-element.109), calls=%async_computation.3 | async-start | bytes 524288 | tf_op jit(solution)/shard_map/all_to_all | solution.py:225
  217.6 0.7 copy-start.85
  (41 other events, 25.1 us)
